TPU v7x, 32 devices: a whole 2x2x4 slice. The times are simulated.
32 devices in a mesh: rep: 2 (over x), fs: 8 (over z, y), tp: 2 (over core).
Axes of the slice: x: 2, y: 2, z: 4, core: 2. Of those that a mesh axis runs over, the one named last changes fastest.
Arguments:
- tokens: bfloat16 [16, 64, 2048], P(('rep', 'fs'), None, 'tp'), may hold values from -6 to 6
- lin_weight: bfloat16 [2048, 1024], P('fs', 'tp'), may hold values from -0.125 to 0.125
- glu_weight: bfloat16 [2048, 1024], P('fs', 'tp'), may hold values from -0.125 to 0.125
- conv_taps: float32 [31, 1024], P(None, 'tp'), may hold values from -4 to 4
- conv_gain: float32 [1024], P('tp'), may hold values from 0.1 to 1.9
- conv_out_weight: bfloat16 [1024, 2048], P('tp', 'fs'), may hold values from -0.1875 to 0.1875
- mix_gain: float32 [2048], replicated, may hold values from 0.1 to 1.9
- ff_gate: bfloat16 [2048, 5632], P('fs', 'tp'), may hold values from -0.125 to 0.125
- ff_up: bfloat16 [2048, 5632], P('fs', 'tp'), may hold values from -0.125 to 0.125
- ff_down: bfloat16 [5632, 2048], P('tp', 'fs'), may hold values from -0.078125 to 0.078125
- out_gain: float32 [2048], replicated, may hold values from 0.1 to 1.9
Outputs:
- encoded: bfloat16 [16, 64, 2048], P(('rep', 'fs'), None, 'tp')
All inputs are finite; a program needn't handle non-finite values.
Results may differ from a plain program's by a relative error of at most 0.014.
Values may be sent and summed in bfloat16 or wider, within the bound.
A program may use at most 128 MiB of HBM per device.

v0:
```python
import jax
import jax.numpy as jnp
from jax import lax
from jax.sharding import PartitionSpec as P

residual_scale = 2.0**0.25
epsilon = 1e-05


def normed(values):
    average = jnp.mean(values, axis=-1, keepdims=True)
    second = jnp.mean(values * values, axis=-1, keepdims=True)
    return (values - average) * lax.rsqrt(second - average * average + epsilon)


def interleave(left, right, parts):
    rows, width = left.shape
    pair = jnp.concatenate(
        (left.reshape(rows, parts, width // parts), right.reshape(rows, parts, width // parts)),
        axis=2,
    )
    return pair.reshape(rows, 2 * width)


def on_device(
    tokens,
    lin_weight,
    glu_weight,
    conv_taps,
    conv_gain_all,
    conv_out_weight,
    mix_gain,
    ff_gate,
    ff_up,
    ff_down,
    out_gain,
):
    n_fs, n_tp = (lax.axis_size("fs"), lax.axis_size("tp"))
    fs_index, tp_index = (lax.axis_index("fs"), lax.axis_index("tp"))
    seqs, length, feat = tokens.shape
    groups = n_fs * seqs
    rows = groups * length
    model = feat * n_tp
    gathered = lax.all_gather(tokens, ("fs", "tp"), axis=0, tiled=False)
    all_tokens = (
        gathered.reshape(n_fs, n_tp, seqs, length, feat)
        .transpose(0, 2, 3, 1, 4)
        .reshape(rows, model)
    )
    glu_pair = lax.all_to_all(
        interleave(lin_weight, glu_weight, n_fs), "fs", split_axis=1, concat_axis=0, tiled=True
    )
    own_out = lax.all_to_all(conv_out_weight, "tp", split_axis=1, concat_axis=0, tiled=True)
    ff_pair = lax.all_to_all(
        interleave(ff_gate, ff_up, n_fs), "fs", split_axis=1, concat_axis=0, tiled=True
    )
    own_down = lax.all_to_all(ff_down, "fs", split_axis=0, concat_axis=1, tiled=True)
    chans = glu_pair.shape[1] // 2
    product = jnp.dot(all_tokens, glu_pair, preferred_element_type=jnp.float32)
    glu = (product[:, :chans] * jax.nn.sigmoid(product[:, chans:])).astype(jnp.bfloat16)
    n_taps = conv_taps.shape[0]
    margin = (n_taps - 1) // 2
    own_taps = lax.dynamic_slice_in_dim(conv_taps, fs_index * chans, chans, 1)
    padded = jnp.pad(
        glu.astype(jnp.float32).reshape(groups, length, chans), ((0, 0), (margin, margin), (0, 0))
    )
    conv = sum((padded[:, k : k + length] * own_taps[k] for k in range(n_taps)))
    conv = conv.reshape(rows, chans).astype(jnp.bfloat16)
    conv_all = lax.all_gather(conv, ("tp", "fs"), axis=1, tiled=True)
    activated = jax.nn.silu(normed(conv_all.astype(jnp.float32)) * conv_gain_all).astype(
        jnp.bfloat16
    )
    mixed_own = jnp.dot(activated, own_out, preferred_element_type=jnp.float32).astype(jnp.bfloat16)
    mixed = lax.all_gather(mixed_own, ("fs", "tp"), axis=1, tiled=True)
    before = residual_scale * all_tokens.astype(jnp.float32) + mixed.astype(jnp.float32)
    middle = (normed(before) * mix_gain).astype(jnp.bfloat16)
    units = ff_pair.shape[1] // 2
    both = jnp.dot(middle, ff_pair, preferred_element_type=jnp.float32)
    hidden = (jax.nn.silu(both[:, :units]) * both[:, units:]).astype(jnp.bfloat16)
    down = jnp.dot(hidden, own_down, preferred_element_type=jnp.float32).astype(jnp.bfloat16)
    sends = (
        down.reshape(n_fs, seqs * length, n_tp, feat)
        .transpose(0, 2, 1, 3)
        .reshape(n_fs * n_tp, seqs * length, feat)
    )
    arrived = lax.all_to_all(sends, ("fs", "tp"), split_axis=0, concat_axis=0, tiled=True)
    forward = jnp.sum(arrived.astype(jnp.float32), axis=0)
    forward = forward.astype(jnp.bfloat16).astype(jnp.float32)
    middle_own = lax.dynamic_slice(
        middle, (fs_index * seqs * length, tp_index * feat), (seqs * length, feat)
    )
    final = residual_scale * middle_own.astype(jnp.float32) + forward
    sums, squares = lax.psum(
        (jnp.sum(final, axis=1, keepdims=True), jnp.sum(final * final, axis=1, keepdims=True)), "tp"
    )
    average = sums / model
    out = (final - average) * lax.rsqrt(squares / model - average * average + epsilon)
    gain = lax.dynamic_slice_in_dim(out_gain, tp_index * feat, feat, 0)
    return (out * gain).astype(jnp.bfloat16).reshape(seqs, length, feat)


def solution(mesh):
    mapped = jax.shard_map(
        on_device,
        mesh=mesh,
        in_specs=(
            P(("rep", "fs"), None, "tp"),
            P("fs", "tp"),
            P("fs", "tp"),
            P(None, "tp"),
            P(),
            P("tp", "fs"),
            P(),
            P("fs", "tp"),
            P("fs", "tp"),
            P("tp", "fs"),
            P(),
        ),
        out_specs=P(("rep", "fs"), None, "tp"),
        check_vma=False,
    )
    return mapped
```

profile of v0, /device:TPU:17, one launch (start us, length us, event | category | flops | bytes accessed | tf_op | source)
XLA Modules:
  0.0 278.2 jit_solution(18404688022100981771)
XLA Ops:
  6.5 0.7 all-gather.11.cloned.1.call-update
  7.3 1.1 copy.34
  8.3 1.1 copy.35
  9.4 0.8 pad_maximum_fusion.1
  10.3 5.6 %all-to-all-start = ((bf16[256,8,128]{0,2,1:T(8,128)(2,1)}), bf16[256,8,128]{0,2,1:T(8,128)(2,1)S(1)}, u32[]{:S(2)}, u32[]{:S(2)}) async-start(bf16[256,8,128]{0,2,1:T(8,128)(2,1)} %pad_maximum_fusion.1), calls=%async_computation | async-start | bytes 1048576 | tf_op jit(solution)/shard_map/all_to_all | solution.py:50
  15.9 0.8 copy.37
  16.7 1.6 dynamic-slice_bitcast_fusion.29
  18.4 1.8 dynamic-slice_bitcast_fusion.30
  20.2 11.9 %all-to-all-done = bf16[256,8,128]{0,2,1:T(8,128)(2,1)S(1)} async-done(((bf16[256,8,128]{0,2,1:T(8,128)(2,1)}), bf16[256,8,128]{0,2,1:T(8,128)(2,1)S(1)}, u32[]{:S(2)}, u32[]{:S(2)}) %all-to-all-start) | async-done | bytes 524320 | tf_op jit(solution)/shard_map/all_to_all | solution.py:50
  32.0 4.2 %all-to-all-start.1 = ((bf16[512,2,128]{0,2,1:T(8,128)(2,1)}), bf16[512,2,128]{0,2,1:T(8,128)(2,1)S(1)}, u32[]{:S(2)}, u32[]{:S(2)}) async-start(bf16[512,2,128]{0,2,1:T(8,128)(2,1)} %bitcast.40), calls=%async_computation.1 | async-start | bytes 524288 | tf_op jit(solution)/shard_map/all_to_all | solution.py:53
  36.2 1.0 copy.36
  37.2 16.4 %all-gather.11.cloned.1.call-done = bf16[16,64,1024]{2,1,0:T(8,128)(2,1)} async-done(((bf16[1,64,1024]{2,1,0:T(8,128)(2,1)}), bf16[16,64,1024]{2,1,0:T(8,128)(2,1)}) %all-gather.11.cloned.1.call-update) | async-done | bytes 2097168 | tf_op jit(solution)/shard_map/all_gather | solution.py:44
  53.7 3.7 %copy.33 = bf16[8,2,1,64,1024]{4,1,3,0,2:T(2,128)(2,1)S(1)} copy(bf16[8,2,1,64,1024]{4,3,1,0,2:T(8,128)(2,1)} %bitcast.118) | data formatting | bytes 4194304 | tf_op jit(solution)/shard_map/reshape | solution.py:46
  57.4 0.6 copy.46
  58.0 0.7 copy-done.4
  58.8 5.5 %all-to-all-start.3 = ((bf16[8,352,256]{2,1,0:T(8,128)(2,1)}), bf16[8,352,256]{2,1,0:T(8,128)(2,1)S(1)}, u32[]{:S(2)}, u32[]{:S(2)}) async-start(bf16[8,352,256]{2,1,0:T(8,128)(2,1)} %bitcast.121), calls=%async_computation.3 | async-start | bytes 2883584 | tf_op jit(solution)/shard_map/all_to_all | solution.py:57
  64.3 1.9 convolution_bitcast_fusion
  66.1 0.7 fusion.36
  66.8 1.7 reshape.133
  68.6 12.1 %add_convert_fusion = bf16[8,64,64]{1,0,2:T(8,128)(2,1)} fusion(f32[8,64,64]{1,0,2:T(8,128)} %reshape.133, f32[64]{0:T(128)} %get-tuple-element.43, f32[64]{0:T(128)S(1)} %get-tuple-element.14, f32[64]{0:T(128)S(1)} %get-tuple-element.15, f32[64]{0:T(128)S(1)} %get-tuple-element.16, f32[64]{0:T(128)} %get-tuple-element.17, f32[64]{0:T(128)} %get-tuple-element.18, ...), kind=kLoop, calls=%fused_computation.27 | loop fusion | flops 2031616 | bytes 204544 | tf_op jit(solution)/shard_map/convert_element_type | solution.py:68
  80.6 1.7 convert_element_type.50
  82.4 2.6 copy.39
  84.9 2.5 copy.40
  87.5 3.6 %pad_maximum_fusion = bf16[256,8,704]{0,2,1:T(8,128)(2,1)} fusion(bf16[256,8,352]{0,2,1:T(8,128)(2,1)} %bitcast.116, bf16[256,8,352]{0,2,1:T(8,128)(2,1)} %bitcast.115), kind=kLoop, calls=%fused_computation.8 | loop fusion | flops 5767168 | bytes 5767168 | tf_op jit(solution)/shard_map/concatenate | solution.py:18
  91.0 5.2 %all-to-all-done.3 = bf16[8,352,256]{2,1,0:T(8,128)(2,1)S(1)} async-done(((bf16[8,352,256]{2,1,0:T(8,128)(2,1)}), bf16[8,352,256]{2,1,0:T(8,128)(2,1)S(1)}, u32[]{:S(2)}, u32[]{:S(2)}) %all-to-all-start.3) | async-done | bytes 1441824 | tf_op jit(solution)/shard_map/all_to_all | solution.py:57
  96.2 7.6 %all-to-all-start.2 = ((bf16[256,8,704]{0,2,1:T(8,128)(2,1)}), bf16[256,8,704]{0,2,1:T(8,128)(2,1)}, u32[]{:S(2)}, u32[]{:S(2)}) async-start(bf16[256,8,704]{0,2,1:T(8,128)(2,1)} %pad_maximum_fusion), calls=%async_computation.2 | async-start | bytes 5767168 | tf_op jit(solution)/shard_map/all_to_all | solution.py:54
  103.8 1.8 copy.38
  105.6 3.2 %all-gather.2 = f32[2,1,512]{2,1,0:T(1,128)S(1)} all-gather(f32[1,1,512]{2,1,0:T(1,128)S(1)} %bitcast.128), channel_id=3, replica_groups=mesh['rep'=2,'fs'=8,'tp'=2] {'tp'}, dimensions={0}, use_global_device_ids=true | all-gather | bytes 6144 | tf_op args[4]
  108.8 19.7 %all-gather.7.cloned.1.call-done = bf16[512,1024]{0,1:T(8,128)(2,1)} async-done(((bf16[512,64]{0,1:T(8,128)(2,1)}), bf16[512,1024]{0,1:T(8,128)(2,1)}) %all-gather.7.cloned.1.call-update) | async-done | bytes 1048592 | tf_op jit(solution)/shard_map/all_gather | solution.py:69
  128.5 1.6 convert_reduce_fusion
  130.0 2.9 %convolution_convert_fusion.1 = bf16[512,128]{1,0:T(8,128)(2,1)} fusion(bf16[1024,128]{1,0:T(8,128)(2,1)} %bitcast.126, bf16[512,1024]{0,1:T(8,128)(2,1)} %all-gather.7.cloned.1.call-done, f32[1024]{0:T(1024)S(1)} %bitcast.127, f32[512]{0:T(512)S(1)} %get-tuple-element.47, f32[512]{0:T(512)S(1)} %get-tuple-element.46), kind=kOutput, calls=%fused_computation.19 | convolution fusion | flops 139001856 | bytes 1449984 | tf_op jit(solution)/shard_map/dot_general | solution.py:73
  133.0 1.4 copy.45
  134.4 38.2 %all-to-all-done.2 = bf16[256,8,704]{0,2,1:T(8,128)(2,1)} async-done(((bf16[256,8,704]{0,2,1:T(8,128)(2,1)}), bf16[256,8,704]{0,2,1:T(8,128)(2,1)}, u32[]{:S(2)}, u32[]{:S(2)}) %all-to-all-start.2) | async-done | bytes 2883616 | tf_op jit(solution)/shard_map/all_to_all | solution.py:54
  172.6 3.8 %copy.44 = bf16[8,88,8,256]{3,2,0,1:T(8,128)(2,1)} copy(bf16[8,88,8,256]{3,2,1,0:T(8,128)(2,1)} %bitcast.56) | data formatting | bytes 5767168 | tf_op jit(solution)/shard_map/all_to_all | solution.py:54
  176.4 22.5 %all-gather.9.cloned.1.call-done = bf16[512,2048]{1,0:T(8,128)(2,1)} async-done(((bf16[512,128]{1,0:T(8,128)(2,1)}), bf16[512,2048]{1,0:T(8,128)(2,1)}) %all-gather.9.cloned.1.call-update) | async-done | bytes 2097168 | tf_op jit(solution)/shard_map/all_gather | solution.py:74
  198.9 2.8 %fusion = (f32[512]{0:T(512)S(1)}, f32[512]{0:T(512)S(1)}) fusion(bf16[512,2048]{1,0:T(8,128)(2,1)} %all-gather.9.cloned.1.call-done, bf16[512,2048]{1,0:T(8,128)(2,1)S(1)} %bitcast.110), kind=kLoop, calls=%fused_computation.3 | loop fusion | flops 7339008 | bytes 4198400 | tf_op jit(solution)/shard_map/reduce_sum | solution.py:11
  201.7 1.1 multiply_convert_fusion
  202.8 0.7 copy-done.1
  203.5 1.7 fusion.39
  205.2 2.7 convolution_convert_fusion
  207.9 3.3 %reshape.129 = bf16[8,64,2,1024]{3,2,1,0:T(2,128)(2,1)S(1)} reshape(bf16[512,2048]{1,0:T(8,128)(2,1)} %convolution_convert_fusion) | data formatting | bytes 4194304 | tf_op jit(solution)/shard_map/reshape | solution.py:82
  211.2 2.0 copy.43
  213.2 5.2 %all-to-all-start.4 = ((bf16[16,64,1024]{2,1,0:T(8,128)(2,1)}), bf16[16,64,1024]{2,1,0:T(8,128)(2,1)S(1)}, u32[]{:S(2)}, u32[]{:S(2)}) async-start(bf16[16,64,1024]{2,1,0:T(8,128)(2,1)} %bitcast.112), calls=%async_computation.4 | async-start | bytes 4194304 | tf_op jit(solution)/shard_map/all_to_all | solution.py:86
  218.4 47.0 %all-to-all-done.4 = bf16[16,64,1024]{2,1,0:T(8,128)(2,1)S(1)} async-done(((bf16[16,64,1024]{2,1,0:T(8,128)(2,1)}), bf16[16,64,1024]{2,1,0:T(8,128)(2,1)S(1)}, u32[]{:S(2)}, u32[]{:S(2)}) %all-to-all-start.4) | async-done | bytes 2097184 | tf_op jit(solution)/shard_map/all_to_all | solution.py:86
  265.5 0.4 reduce_sum.70
  265.9 1.1 fusion.29
  266.9 3.1 %all-reduce.1 = (f32[64,1]{0,1:T(1,128)S(1)}, f32[64,1]{0,1:T(1,128)S(1)}) all-reduce(f32[64,1]{0,1:T(1,128)S(1)} %bitcast.130, f32[64,1]{0,1:T(1,128)S(1)} %bitcast.129), channel_id=1, replica_groups=mesh['rep'=2,'fs'=8,'tp'=2] {'tp'}, use_global_device_ids=true, to_apply=%region_8.9 | all-reduce | flops 128 | bytes 1024 | tf_op jit(solution)/shard_map/psum | solution.py:93
  270.0 1.7 fusion.30
  (25 shorter events, 0.1 us)
Async XLA Ops:
  6.5 9.3 %copy-start.5 = (bf16[512,256]{1,0:T(8,128)(2,1)S(1)}, bf16[512,256]{1,0:T(8,128)(2,1)}, u32[]{:S(2)}) copy-start(bf16[512,256]{1,0:T(8,128)(2,1)} %param.16) | copy-start | bytes 786436
  6.5 47.1 %all-gather.11.cloned.1.call-start = ((), (), s32[]{:S(2)}) async-start(), calls=%async_computation.7 | async-start | bytes 2228224 | tf_op jit(solution)/shard_map/all_gather | solution.py:44
  10.3 21.7 %all-to-all-start = ((bf16[256,8,128]{0,2,1:T(8,128)(2,1)}), bf16[256,8,128]{0,2,1:T(8,128)(2,1)S(1)}, u32[]{:S(2)}, u32[]{:S(2)}) async-start(bf16[256,8,128]{0,2,1:T(8,128)(2,1)} %pad_maximum_fusion.1), calls=%async_computation | async-start | bytes 1048576 | tf_op jit(solution)/shard_map/all_to_all | solution.py:50
  32.0 26.0 %all-to-all-start.1 = ((bf16[512,2,128]{0,2,1:T(8,128)(2,1)}), bf16[512,2,128]{0,2,1:T(8,128)(2,1)S(1)}, u32[]{:S(2)}, u32[]{:S(2)}) async-start(bf16[512,2,128]{0,2,1:T(8,128)(2,1)} %bitcast.40), calls=%async_computation.1 | async-start | bytes 524288 | tf_op jit(solution)/shard_map/all_to_all | solution.py:53
  58.0 0.7 copy-start.4
  58.8 37.5 %all-to-all-start.3 = ((bf16[8,352,256]{2,1,0:T(8,128)(2,1)}), bf16[8,352,256]{2,1,0:T(8,128)(2,1)S(1)}, u32[]{:S(2)}, u32[]{:S(2)}) async-start(bf16[8,352,256]{2,1,0:T(8,128)(2,1)} %bitcast.121), calls=%async_computation.3 | async-start | bytes 2883584 | tf_op jit(solution)/shard_map/all_to_all | solution.py:57
  64.3 64.2 %all-gather.7.cloned.1.call-start = ((), (), s32[]{:S(2)}) async-start(), calls=%async_computation.5 | async-start | bytes 1114112 | tf_op jit(solution)/shard_map/all_gather | solution.py:69
  91.0 14.6 %copy-start.7 = (f32[512]{0:T(512)S(1)}, f32[512]{0:T(512)}, u32[]{:S(2)}) copy-start(f32[512]{0:T(512)} %param.15) | copy-start | bytes 6148
  96.2 76.3 %all-to-all-start.2 = ((bf16[256,8,704]{0,2,1:T(8,128)(2,1)}), bf16[256,8,704]{0,2,1:T(8,128)(2,1)}, u32[]{:S(2)}, u32[]{:S(2)}) async-start(bf16[256,8,704]{0,2,1:T(8,128)(2,1)} %pad_maximum_fusion), calls=%async_computation.2 | async-start | bytes 5767168 | tf_op jit(solution)/shard_map/all_to_all | solution.py:54
  103.8 95.1 %all-gather.9.cloned.1.call-start = ((), (), s32[]{:S(2)}) async-start(), calls=%async_computation.6 | async-start | bytes 2228224 | tf_op jit(solution)/shard_map/all_gather | solution.py:74
  176.4 25.3 %copy-start.6 = (f32[2048]{0:T(1024)S(1)}, f32[2048]{0:T(1024)}, u32[]{:S(2)}) copy-start(f32[2048]{0:T(1024)} %param.17) | copy-start | bytes 24580
  198.9 2.8 %copy-start = (bf16[512,2048]{1,0:T(8,128)(2,1)S(1)}, bf16[512,2048]{1,0:T(8,128)(2,1)}, u32[]{:S(2)}) copy-start(bf16[512,2048]{1,0:T(8,128)(2,1)} %all-gather.9.cloned.1.call-done) | copy-start | bytes 6291460
  201.7 1.8 copy-start.1
  202.8 2.4 copy-start.2
  203.5 1.7 copy-start.3
  213.2 52.3 %all-to-all-start.4 = ((bf16[16,64,1024]{2,1,0:T(8,128)(2,1)}), bf16[16,64,1024]{2,1,0:T(8,128)(2,1)S(1)}, u32[]{:S(2)}, u32[]{:S(2)}) async-start(bf16[16,64,1024]{2,1,0:T(8,128)(2,1)} %bitcast.112), calls=%async_computation.4 | async-start | bytes 4194304 | tf_op jit(solution)/shard_map/all_to_all | solution.py:86
  218.4 51.6 %dynamic-slice-start = ((f32[2048]{0:T(1024)}, s32[]{:T(128)}), f32[1024]{0:T(1024)S(1)}, s32[]{:S(2)}) async-start(f32[2048]{0:T(1024)} %param.21, s32[]{:T(128)} %select_n.9), calls=%async_computation.8 | async-start | bytes 8704 | tf_op jit(solution)/shard_map/dynamic_slice | solution.py:98
Sparse Core Ops, SparseCore 0:
  9.5 44.1 all-gather.10
  82.5 45.9 all-gather.6
  133.1 65.7 all-gather.8
where the time goes:
time: 279 us; the launch traced here: 278 us
  waiting for transfers between devices  162 us (58%)
  local copies, waits for them, and re-layouts  34 us (12%)
  starting transfers between devices  28.1 us (10%)
  other arithmetic  25.8 us (9%)
  between operations  13.3 us (5%)
  matrix products  9.17 us (3%)
  blocking collectives  6.25 us (2%)
    all_to_all x1, waiting for transfers between devices, on_device(): lax.all_to_all(sends, ('fs', 'tp'), split_axis=0, concat_axis=0, tiled=True)  47 us
    all_to_all x1, waiting for transfers between devices, on_device(): lax.all_to_all(interleave(ff_gate, ff_up, n_fs), 'fs', split_axis=1, conc...  38.2 us
    all_gather x1, waiting for transfers between devices, on_device(): mixed = lax.all_gather(mixed_own, ('fs', 'tp'), axis=1, tiled=True)  22.5 us
    all_gather x1, waiting for transfers between devices, on_device(): conv_all = lax.all_gather(conv, ('tp', 'fs'), axis=1, tiled=True)  19.7 us
    all_gather x1, waiting for transfers between devices, on_device(): gathered = lax.all_gather(tokens, ('fs', 'tp'), axis=0, tiled=False)  16.4 us
    convert_element_type x1, other arithmetic, on_device(): conv = conv.reshape(rows, chans).astype(jnp.bfloat16)  12.1 us
    all_to_all x1, waiting for transfers between devices, on_device(): lax.all_to_all(interleave(lin_weight, glu_weight, n_fs), 'fs', split_axis...  11.9 us
    unnamed x22, local copies, waits for them, and re-layouts  10.2 us
  transfers between devices with their start and end apart: 8, of which 7 were waited for; matrix products, arithmetic and copies ran while one was open for 18% of the time, Pallas kernels for 0%

commit v1 on v0

--- a/solution.py
+++ b/solution.py
@@ -5,6 +5,12 @@
 
 residual_scale = 2.0**0.25
 epsilon = 1e-05
+
+
+def stacked_exchange(x, axis, split, join):
+    cells = jnp.split(x, lax.axis_size(axis), axis=split)
+    incoming = lax.all_to_all(jnp.stack(cells), axis, 0, 0)
+    return jnp.concatenate(incoming, axis=join)
 
 
 def normed(values):
@@ -51,9 +57,7 @@
         interleave(lin_weight, glu_weight, n_fs), "fs", split_axis=1, concat_axis=0, tiled=True
     )
     own_out = lax.all_to_all(conv_out_weight, "tp", split_axis=1, concat_axis=0, tiled=True)
-    ff_pair = lax.all_to_all(
-        interleave(ff_gate, ff_up, n_fs), "fs", split_axis=1, concat_axis=0, tiled=True
-    )
+    ff_pair = stacked_exchange(interleave(ff_gate, ff_up, n_fs), "fs", 1, 0)
     own_down = lax.all_to_all(ff_down, "fs", split_axis=0, concat_axis=1, tiled=True)
     chans = glu_pair.shape[1] // 2
     product = jnp.dot(all_tokens, glu_pair, preferred_element_type=jnp.float32)

time: 279 us -> 280 us (level)
  local copies, waits for them, and re-layouts: 34 us -> 41.5 us
  waiting for transfers between devices: 162 us -> 156 us
    unnamed x22 -> x35, local copies, waits for them, and re-layouts: 10.2 us -> 16.9 us
    all_to_all x1, waiting for transfers between devices: 11.9 us -> 7.63 us  [on_device(): lax.all_to_all(interleave(lin_weight, glu_weight, n_fs), 'fs', split_axis...]
    all_to_all x1 -> x0, local copies, waits for them, and re-layouts: 3.8 us -> none  [on_device(): lax.all_to_all(interleave(ff_gate, ff_up, n_fs), 'fs', split_axis=1, conc...]
    reshape x0 -> x1, local copies, waits for them, and re-layouts: none -> 3.8 us  [stacked_exchange(): return jnp.concatenate(incoming, axis=join)]
  transfers between devices with their start and end apart: 8 -> 8, of which waited for: 7 -> 7; matrix products, arithmetic and copies ran while one was open for 18% -> 20% of each run, Pallas kernels for 0% -> 0%
where the time goes in v1:
time: 280 us; the launch traced here: 279 us
  waiting for transfers between devices  156 us (56%)
  local copies, waits for them, and re-layouts  41.5 us (15%)
  starting transfers between devices  28.5 us (10%)
  other arithmetic  23.8 us (8%)
  between operations  13.3 us (5%)
  matrix products  9.15 us (3%)
  blocking collectives  6.17 us (2%)
    all_to_all x1, waiting for transfers between devices, on_device(): lax.all_to_all(sends, ('fs', 'tp'), split_axis=0, concat_axis=0, tiled=True)  47 us
    all_to_all x1, waiting for transfers between devices, stacked_exchange(): incoming = lax.all_to_all(jnp.stack(cells), axis, 0, 0)  38.1 us
    all_gather x1, waiting for transfers between devices, on_device(): mixed = lax.all_gather(mixed_own, ('fs', 'tp'), axis=1, tiled=True)  22.4 us
    all_gather x1, waiting for transfers between devices, on_device(): conv_all = lax.all_gather(conv, ('tp', 'fs'), axis=1, tiled=True)  20 us
    unnamed x35, local copies, waits for them, and re-layouts  16.9 us
    all_gather x1, waiting for transfers between devices, on_device(): gathered = lax.all_gather(tokens, ('fs', 'tp'), axis=0, tiled=False)  16.5 us
    convert_element_type x1, other arithmetic, on_device(): conv = conv.reshape(rows, chans).astype(jnp.bfloat16)  11.9 us
    all_to_all x1, starting transfers between devices, stacked_exchange(): incoming = lax.all_to_all(jnp.stack(cells), axis, 0, 0)  7.79 us
  transfers between devices with their start and end apart: 8, of which 7 were waited for; matrix products, arithmetic and copies ran while one was open for 20% of the time, Pallas kernels for 0%

profile of v1, /device:TPU:17, one launch (start us, length us, event | category | flops | bytes accessed | tf_op | source)
XLA Modules:
  0.0 278.5 jit_solution(3357184700737185288)
XLA Ops:
  7.3 1.1 copy.33
  8.3 1.1 copy.34
  9.4 0.8 pad_maximum_fusion.1
  10.3 5.6 %all-to-all-start = ((bf16[256,8,128]{0,2,1:T(8,128)(2,1)}), bf16[256,8,128]{0,2,1:T(8,128)(2,1)S(1)}, u32[]{:S(2)}, u32[]{:S(2)}) async-start(bf16[256,8,128]{0,2,1:T(8,128)(2,1)} %pad_maximum_fusion.1), calls=%async_computation | async-start | bytes 1048576 | tf_op jit(solution)/shard_map/all_to_all | solution.py:56
  15.9 0.8 copy.36
  17.4 1.7 copy.39
  19.2 1.7 dynamic-slice_bitcast_fusion.29
  20.8 1.8 dynamic-slice_bitcast_fusion.30
  22.6 1.8 pad_maximum_fusion
  24.4 7.6 %all-to-all-done = bf16[256,8,128]{0,2,1:T(8,128)(2,1)S(1)} async-done(((bf16[256,8,128]{0,2,1:T(8,128)(2,1)}), bf16[256,8,128]{0,2,1:T(8,128)(2,1)S(1)}, u32[]{:S(2)}, u32[]{:S(2)}) %all-to-all-start) | async-done | bytes 524320 | tf_op jit(solution)/shard_map/all_to_all | solution.py:56
  32.0 4.2 %all-to-all-start.1 = ((bf16[512,2,128]{0,2,1:T(8,128)(2,1)}), bf16[512,2,128]{0,2,1:T(8,128)(2,1)S(1)}, u32[]{:S(2)}, u32[]{:S(2)}) async-start(bf16[512,2,128]{0,2,1:T(8,128)(2,1)} %bitcast.164), calls=%async_computation.1 | async-start | bytes 524288 | tf_op jit(solution)/shard_map/all_to_all | solution.py:59
  36.2 1.0 copy.35
  37.3 16.5 %all-gather.11.cloned.1.call-done = bf16[16,64,1024]{2,1,0:T(8,128)(2,1)} async-done(((bf16[1,64,1024]{2,1,0:T(8,128)(2,1)}), bf16[16,64,1024]{2,1,0:T(8,128)(2,1)}) %all-gather.11.cloned.1.call-update) | async-done | bytes 2097168 | tf_op jit(solution)/shard_map/all_gather | solution.py:50
  53.8 3.7 %copy.32 = bf16[8,2,1,64,1024]{4,1,3,0,2:T(2,128)(2,1)S(1)} copy(bf16[8,2,1,64,1024]{4,3,1,0,2:T(8,128)(2,1)} %bitcast.158) | data formatting | bytes 4194304 | tf_op jit(solution)/shard_map/reshape | solution.py:52
  58.9 5.5 %all-to-all-start.3 = ((bf16[8,352,256]{2,1,0:T(8,128)(2,1)}), bf16[8,352,256]{2,1,0:T(8,128)(2,1)S(1)}, u32[]{:S(2)}, u32[]{:S(2)}) async-start(bf16[8,352,256]{2,1,0:T(8,128)(2,1)} %bitcast.161), calls=%async_computation.3 | async-start | bytes 2883584 | tf_op jit(solution)/shard_map/all_to_all | solution.py:61
  64.4 1.9 convolution_bitcast_fusion
  67.0 1.7 reshape.136
  68.7 11.9 %add_convert_fusion = bf16[8,64,64]{1,0,2:T(8,128)(2,1)} fusion(f32[8,64,64]{1,0,2:T(8,128)} %reshape.136, f32[64]{0:T(128)} %get-tuple-element.43, f32[64]{0:T(128)S(1)} %get-tuple-element.14, f32[64]{0:T(128)S(1)} %get-tuple-element.15, f32[64]{0:T(128)S(1)} %get-tuple-element.16, f32[64]{0:T(128)} %get-tuple-element.17, f32[64]{0:T(128)} %get-tuple-element.18, ...), kind=kLoop, calls=%fused_computation.43 | loop fusion | flops 2031616 | bytes 204544 | tf_op jit(solution)/shard_map/convert_element_type | solution.py:72
  80.6 1.7 convert_element_type.50
  82.3 1.9 fusion.20
  84.2 1.8 fusion.19
  86.0 1.8 fusion.18
  87.7 1.7 fusion.17
  90.2 0.8 fusion.15
  91.0 0.8 fusion.14
  91.8 0.8 fusion.13
  92.5 3.6 %all-to-all-done.3 = bf16[8,352,256]{2,1,0:T(8,128)(2,1)S(1)} async-done(((bf16[8,352,256]{2,1,0:T(8,128)(2,1)}), bf16[8,352,256]{2,1,0:T(8,128)(2,1)S(1)}, u32[]{:S(2)}, u32[]{:S(2)}) %all-to-all-start.3) | async-done | bytes 1441824 | tf_op jit(solution)/shard_map/all_to_all | solution.py:61
  96.2 7.8 %all-to-all-start.2 = ((bf16[8,256,704]{1,2,0:T(8,128)(2,1)}), bf16[8,256,704]{1,2,0:T(8,128)(2,1)}, u32[]{:S(2)}, u32[]{:S(2)}) async-start(bf16[8,256,704]{1,2,0:T(8,128)(2,1)} %fusion.13), calls=%async_computation.2 | async-start | bytes 5767168 | tf_op jit(solution)/shard_map/all_to_all | solution.py:12
  104.0 1.8 copy.37
  105.8 3.1 %all-gather.2 = f32[2,1,512]{2,1,0:T(1,128)S(1)} all-gather(f32[1,1,512]{2,1,0:T(1,128)S(1)} %bitcast.169), channel_id=3, replica_groups=mesh['rep'=2,'fs'=8,'tp'=2] {'tp'}, dimensions={0}, use_global_device_ids=true | all-gather | bytes 6144 | tf_op args[4]
  108.8 20.0 %all-gather.7.cloned.1.call-done = bf16[512,1024]{0,1:T(8,128)(2,1)} async-done(((bf16[512,64]{0,1:T(8,128)(2,1)}), bf16[512,1024]{0,1:T(8,128)(2,1)}) %all-gather.7.cloned.1.call-update) | async-done | bytes 1048592 | tf_op jit(solution)/shard_map/all_gather | solution.py:73
  128.9 1.6 convert_reduce_fusion
  130.4 2.9 %convolution_convert_fusion.1 = bf16[512,128]{1,0:T(8,128)(2,1)} fusion(bf16[1024,128]{1,0:T(8,128)(2,1)} %bitcast.167, bf16[512,1024]{0,1:T(8,128)(2,1)} %all-gather.7.cloned.1.call-done, f32[1024]{0:T(1024)S(1)} %bitcast.168, f32[512]{0:T(512)S(1)} %get-tuple-element.47, f32[512]{0:T(512)S(1)} %get-tuple-element.46), kind=kOutput, calls=%fused_computation.19 | convolution fusion | flops 139001856 | bytes 1449984 | tf_op jit(solution)/shard_map/dot_general | solution.py:77
  133.4 1.4 copy.44
  134.8 38.1 %all-to-all-done.2 = bf16[8,256,704]{1,2,0:T(8,128)(2,1)} async-done(((bf16[8,256,704]{1,2,0:T(8,128)(2,1)}), bf16[8,256,704]{1,2,0:T(8,128)(2,1)}, u32[]{:S(2)}, u32[]{:S(2)}) %all-to-all-start.2) | async-done | bytes 2883616 | tf_op jit(solution)/shard_map/all_to_all | solution.py:12
  172.8 3.8 %copy.43 = bf16[8,88,8,256]{3,2,0,1:T(8,128)(2,1)} copy(bf16[8,88,8,256]{3,2,1,0:T(8,128)(2,1)} %bitcast.64) | data formatting | bytes 5767168 | tf_op jit(solution)/shard_map/reshape | solution.py:13
  176.7 22.4 %all-gather.9.cloned.1.call-done = bf16[512,2048]{1,0:T(8,128)(2,1)} async-done(((bf16[512,128]{1,0:T(8,128)(2,1)}), bf16[512,2048]{1,0:T(8,128)(2,1)}) %all-gather.9.cloned.1.call-update) | async-done | bytes 2097168 | tf_op jit(solution)/shard_map/all_gather | solution.py:78
  199.1 2.8 %fusion = (f32[512]{0:T(512)S(1)}, f32[512]{0:T(512)S(1)}) fusion(bf16[512,2048]{1,0:T(8,128)(2,1)} %all-gather.9.cloned.1.call-done, bf16[512,2048]{1,0:T(8,128)(2,1)S(1)} %bitcast.142), kind=kLoop, calls=%fused_computation.3 | loop fusion | flops 7339008 | bytes 4198400 | tf_op jit(solution)/shard_map/reduce_sum | solution.py:17
  201.9 1.1 multiply_convert_fusion
  203.7 1.7 fusion.47
  205.4 2.7 convolution_convert_fusion
  208.1 3.3 %reshape.132 = bf16[8,64,2,1024]{3,2,1,0:T(2,128)(2,1)S(1)} reshape(bf16[512,2048]{1,0:T(8,128)(2,1)} %convolution_convert_fusion) | data formatting | bytes 4194304 | tf_op jit(solution)/shard_map/reshape | solution.py:86
  211.4 2.0 copy.42
  213.3 5.3 %all-to-all-start.4 = ((bf16[16,64,1024]{2,1,0:T(8,128)(2,1)}), bf16[16,64,1024]{2,1,0:T(8,128)(2,1)S(1)}, u32[]{:S(2)}, u32[]{:S(2)}) async-start(bf16[16,64,1024]{2,1,0:T(8,128)(2,1)} %bitcast.152), calls=%async_computation.4 | async-start | bytes 4194304 | tf_op jit(solution)/shard_map/all_to_all | solution.py:90
  218.7 47.0 %all-to-all-done.4 = bf16[16,64,1024]{2,1,0:T(8,128)(2,1)S(1)} async-done(((bf16[16,64,1024]{2,1,0:T(8,128)(2,1)}), bf16[16,64,1024]{2,1,0:T(8,128)(2,1)S(1)}, u32[]{:S(2)}, u32[]{:S(2)}) %all-to-all-start.4) | async-done | bytes 2097184 | tf_op jit(solution)/shard_map/all_to_all | solution.py:90
  266.1 1.1 fusion.37
  267.2 3.1 %all-reduce.1 = (f32[64,1]{0,1:T(1,128)S(1)}, f32[64,1]{0,1:T(1,128)S(1)}) all-reduce(f32[64,1]{0,1:T(1,128)S(1)} %bitcast.171, f32[64,1]{0,1:T(1,128)S(1)} %bitcast.170), channel_id=1, replica_groups=mesh['rep'=2,'fs'=8,'tp'=2] {'tp'}, use_global_device_ids=true, to_apply=%region_8.9 | all-reduce | flops 128 | bytes 1024 | tf_op jit(solution)/shard_map/psum | solution.py:97
  270.3 1.7 fusion.38
  (38 shorter events, 5.4 us)
Async XLA Ops:
  6.5 9.4 %copy-start.7 = (bf16[512,256]{1,0:T(8,128)(2,1)S(1)}, bf16[512,256]{1,0:T(8,128)(2,1)}, u32[]{:S(2)}) copy-start(bf16[512,256]{1,0:T(8,128)(2,1)} %param.16) | copy-start | bytes 786436
  6.5 10.2 %copy-start.4 = (bf16[256,2816]{1,0:T(8,128)(2,1)S(1)}, bf16[256,2816]{1,0:T(8,128)(2,1)}, u32[]{:S(2)}) copy-start(bf16[256,2816]{1,0:T(8,128)(2,1)} %param.18) | copy-start | bytes 4325380
  6.5 47.2 %all-gather.11.cloned.1.call-start = ((), (), s32[]{:S(2)}) async-start(), calls=%async_computation.7 | async-start | bytes 2228224 | tf_op jit(solution)/shard_map/all_gather | solution.py:50
  10.3 21.7 %all-to-all-start = ((bf16[256,8,128]{0,2,1:T(8,128)(2,1)}), bf16[256,8,128]{0,2,1:T(8,128)(2,1)S(1)}, u32[]{:S(2)}, u32[]{:S(2)}) async-start(bf16[256,8,128]{0,2,1:T(8,128)(2,1)} %pad_maximum_fusion.1), calls=%async_computation | async-start | bytes 1048576 | tf_op jit(solution)/shard_map/all_to_all | solution.py:56
  32.0 26.1 %all-to-all-start.1 = ((bf16[512,2,128]{0,2,1:T(8,128)(2,1)}), bf16[512,2,128]{0,2,1:T(8,128)(2,1)S(1)}, u32[]{:S(2)}, u32[]{:S(2)}) async-start(bf16[512,2,128]{0,2,1:T(8,128)(2,1)} %bitcast.164), calls=%async_computation.1 | async-start | bytes 524288 | tf_op jit(solution)/shard_map/all_to_all | solution.py:59
  58.1 0.7 copy-start.6
  58.9 37.3 %all-to-all-start.3 = ((bf16[8,352,256]{2,1,0:T(8,128)(2,1)}), bf16[8,352,256]{2,1,0:T(8,128)(2,1)S(1)}, u32[]{:S(2)}, u32[]{:S(2)}) async-start(bf16[8,352,256]{2,1,0:T(8,128)(2,1)} %bitcast.161), calls=%async_computation.3 | async-start | bytes 2883584 | tf_op jit(solution)/shard_map/all_to_all | solution.py:61
  64.4 64.5 %all-gather.7.cloned.1.call-start = ((), (), s32[]{:S(2)}) async-start(), calls=%async_computation.5 | async-start | bytes 1114112 | tf_op jit(solution)/shard_map/all_gather | solution.py:73
  82.3 7.2 %copy-start = (bf16[256,8,704]{0,2,1:T(8,128)(2,1)S(1)}, bf16[256,8,704]{0,2,1:T(8,128)(2,1)}, u32[]{:S(2)}) copy-start(bf16[256,8,704]{0,2,1:T(8,128)(2,1)} %pad_maximum_fusion) | copy-start | bytes 8650756
  92.5 13.2 %copy-start.9 = (f32[512]{0:T(512)S(1)}, f32[512]{0:T(512)}, u32[]{:S(2)}) copy-start(f32[512]{0:T(512)} %param.15) | copy-start | bytes 6148
  96.2 76.7 %all-to-all-start.2 = ((bf16[8,256,704]{1,2,0:T(8,128)(2,1)}), bf16[8,256,704]{1,2,0:T(8,128)(2,1)}, u32[]{:S(2)}, u32[]{:S(2)}) async-start(bf16[8,256,704]{1,2,0:T(8,128)(2,1)} %fusion.13), calls=%async_computation.2 | async-start | bytes 5767168 | tf_op jit(solution)/shard_map/all_to_all | solution.py:12
  104.0 95.1 %all-gather.9.cloned.1.call-start = ((), (), s32[]{:S(2)}) async-start(), calls=%async_computation.6 | async-start | bytes 2228224 | tf_op jit(solution)/shard_map/all_gather | solution.py:78
  176.7 25.2 %copy-start.8 = (f32[2048]{0:T(1024)S(1)}, f32[2048]{0:T(1024)}, u32[]{:S(2)}) copy-start(f32[2048]{0:T(1024)} %param.17) | copy-start | bytes 24580
  199.1 2.8 %copy-start.1 = (bf16[512,2048]{1,0:T(8,128)(2,1)S(1)}, bf16[512,2048]{1,0:T(8,128)(2,1)}, u32[]{:S(2)}) copy-start(bf16[512,2048]{1,0:T(8,128)(2,1)} %all-gather.9.cloned.1.call-done) | copy-start | bytes 6291460
  201.9 1.8 copy-start.2
  202.9 2.5 copy-start.3
  203.7 1.7 copy-start.5
  213.3 5.3 %copy-start.10 = (f32[2048]{0:T(1024)S(1)}, f32[2048]{0:T(1024)}, u32[]{:S(2)}) copy-start(f32[2048]{0:T(1024)} %param.21) | copy-start | bytes 24580
  213.3 52.4 %all-to-all-start.4 = ((bf16[16,64,1024]{2,1,0:T(8,128)(2,1)}), bf16[16,64,1024]{2,1,0:T(8,128)(2,1)S(1)}, u32[]{:S(2)}, u32[]{:S(2)}) async-start(bf16[16,64,1024]{2,1,0:T(8,128)(2,1)} %bitcast.152), calls=%async_computation.4 | async-start | bytes 4194304 | tf_op jit(solution)/shard_map/all_to_all | solution.py:90
Sparse Core Ops, SparseCore 0:
  9.5 44.2 all-gather.10
  82.4 46.3 all-gather.6
  133.5 65.4 all-gather.8
